TPU v7x, 512 devices: a whole 4x8x8 slice. The times are simulated.
512 devices in a mesh: ep: 32 (over z, x), tp: 16 (over y, core).
Axes of the slice: x: 4, y: 8, z: 8, core: 2. Of those that a mesh axis runs over, the one named last changes fastest.
Arguments:
- tokens_a: bfloat16 [4096, 2048], P('ep'), may hold values from -6 to 6
- gain_a: float32 [2048], replicated, may hold values from 0.1 to 1.9
- value_w: bfloat16 [2048, 2048], P(None, 'tp'), may hold values from -0.125 to 0.125
- gate_w: bfloat16 [2048, 2048], P(None, 'tp'), may hold values from -0.125 to 0.125
- kernel: float32 [31, 2048], P(None, 'tp')
- chan_gain: float32 [2048], P('tp'), may hold values from 0.1 to 1.9
- out_w: bfloat16 [2048, 2048], P('tp'), may hold values from -0.125 to 0.125
- tokens_b: bfloat16 [6144, 2048], P('ep'), may hold values from -6 to 6
- gain_b: float32 [2048], replicated, may hold values from 0.1 to 1.9
- routes: int32 [6144, 2], P('ep'), may hold values from 0 to 31, all different within a row; in each aligned block of 192 rows (0 to 191, 192 to 383, ...) at most 18 rows name the same one
- route_logits: float32 [6144, 2], P('ep'), may hold values from -6 to 6
- expert_gate: bfloat16 [32, 2048, 2816], P('ep', None, 'tp'), may hold values from -0.125 to 0.125
- expert_up: bfloat16 [32, 2048, 2816], P('ep', None, 'tp'), may hold values from -0.125 to 0.125
- expert_down: bfloat16 [32, 2816, 2048], P('ep', 'tp'), may hold values from -0.109375 to 0.109375
Outputs:
- conv_out: bfloat16 [2048, 4096], P('tp', 'ep')
- moe_out: bfloat16 [2048, 6144], P('tp', 'ep')
Inputs may be any that keep to these rules, and one draw needn't show every extreme that they name: `routes`: each row names 2 different experts; among the rows of one index of ep no expert is named by more than 18 rows, a bound that some block reaches.
All inputs are finite; a program needn't handle non-finite values.
Results may differ from a plain program's by a relative error of at most 0.018.
Values may be sent and summed in bfloat16 or wider, within the bound.
A program may use at most 64 MiB of HBM per device.

v0:
```python
import jax
import jax.numpy as jnp
from jax import lax
from jax.sharding import Mesh
from jax.sharding import PartitionSpec as P

CONV_CH = 2048
TP = ("tp_0", "tp_1")


def from_behind(block, axis, distance):
    devices = range(lax.axis_size(axis))
    route = [(i - distance, i) for i in devices if i - distance in devices]
    return lax.ppermute(block, axis, route)


def copy_for_each(x, axis):
    peers = lax.axis_size(axis)
    return lax.all_to_all(jnp.broadcast_to(x[None], (peers, *x.shape)), axis, 0, 0, tiled=True)


def taken_together(x, axis):
    return copy_for_each(x, axis).sum(axis=0)


def in_one(arrays, axis):
    ends = [0]
    for a in arrays:
        ends.append(ends[-1] + a.size)
    so_far = taken_together(jnp.concatenate([a.ravel() for a in arrays]), axis)
    return tuple((so_far[b:e].reshape(a.shape) for a, b, e in zip(arrays, ends, ends[1:])))


def in_blocks(x, dim, peers):
    before, after = (x.shape[:dim], x.shape[dim + 1 :])
    return jnp.moveaxis(x.reshape(*before, peers, -1, *after), dim, 0)


def sum_at_owner(x, axis, dim):
    peers = lax.axis_size(axis)
    tiles = lax.all_to_all(in_blocks(x, dim, peers), axis, 0, 0, tiled=True)
    return jnp.sum(tiles.astype(jnp.float32), axis=0)


def summed_rows(terms, axes):
    so_far = terms.astype(jnp.bfloat16)
    for axis in axes:
        so_far = lax.psum_scatter(so_far, axis, scatter_dimension=0, tiled=True)
    return so_far.astype(jnp.float32)


def rms_scaled(tokens, gain):
    values = tokens.astype(jnp.float32)
    scaled = values * lax.rsqrt(jnp.mean(values * values, axis=1, keepdims=True) + 1e-06)
    return (scaled * gain[None, :]).astype(jnp.bfloat16)


def slot_table(route_rows, experts, capacity):
    flat_expert = route_rows.reshape(-1)
    expert_ids = jnp.arange(experts, dtype=jnp.int32)
    onehot = (flat_expert[:, None] == expert_ids[None, :]).astype(jnp.int32)
    before = jnp.cumsum(onehot, axis=0) - onehot
    ranking = jnp.sum(before * onehot, axis=1)
    return flat_expert * capacity + ranking


def body(
    tokens_a,
    gain_a,
    value_w,
    gate_w,
    kernel,
    chan_gain,
    out_w,
    tokens_b,
    gain_b,
    routes,
    route_logits,
    expert_gate,
    expert_up,
    expert_down,
):
    normed = rms_scaled(tokens_a, gain_a)
    contract_first = (((0,), (1,)), ((), ()))
    value_part = lax.dot_general(
        value_w, normed, contract_first, preferred_element_type=jnp.float32
    )
    gate_part = lax.dot_general(gate_w, normed, contract_first, preferred_element_type=jnp.float32)
    glu = (value_part * jax.nn.sigmoid(gate_part)).astype(jnp.bfloat16)
    taps = kernel.shape[0]
    length = glu.shape[1]
    rim = from_behind(glu[:, length - (taps - 1) :], "ep", 1)
    padded = jnp.concatenate([rim, glu], axis=1).astype(jnp.float32)
    mixed = jnp.zeros(glu.shape, jnp.float32)
    for tap in range(taps):
        mixed = mixed + kernel[tap][:, None] * padded[:, tap : tap + length]
    chan_total, chan_square = in_one((jnp.sum(mixed, axis=0), jnp.sum(mixed * mixed, axis=0)), TP)
    average = chan_total / CONV_CH
    spread = chan_square / CONV_CH - average * average
    normal_out = (
        (mixed - average[None, :]) * lax.rsqrt(spread + 1e-05)[None, :] * chan_gain[:, None]
    )
    activated = jax.nn.silu(normal_out).astype(jnp.bfloat16)
    block_w = out_w
    conv_out = sum_at_owner(
        lax.dot_general(
            block_w, activated, (((0,), (0,)), ((), ())), preferred_element_type=jnp.float32
        ).astype(jnp.bfloat16),
        TP,
        0,
    ).astype(jnp.bfloat16)
    normed_b = rms_scaled(tokens_b, gain_b)
    experts = lax.axis_size("ep")
    token_count = tokens_b.shape[0]
    choices_per = routes.shape[1]
    capacity = 3 * token_count * choices_per // (2 * experts)
    slots = slot_table(routes, experts, capacity)
    owner = jnp.arange(slots.shape[0], dtype=jnp.int32) // choices_per
    filled = jnp.zeros((experts * capacity,), jnp.int32).at[slots].set(owner + 1)
    own = lax.axis_index(TP)
    width = normed_b.shape[1] // lax.axis_size(TP)
    part = lax.dynamic_slice_in_dim(normed_b, own * width, width, axis=1)
    picked = jnp.take(part, jnp.maximum(filled - 1, 0), axis=0)
    send_rows = jnp.where((filled > 0)[:, None], picked, jnp.zeros_like(picked)).reshape(
        experts, capacity, -1
    )
    weights = jax.nn.softmax(route_logits, axis=1).reshape(-1)
    slot_ids = jnp.arange(experts * capacity, dtype=jnp.int32)
    combine = (
        ((slots[:, None] == slot_ids[None, :]).astype(jnp.float32) * weights[:, None])
        .reshape(token_count, choices_per, -1)
        .sum(axis=1)
    )
    gate_local = expert_gate[0]
    up_local = expert_up[0]
    arrived = lax.all_to_all(send_rows, "ep", split_axis=0, concat_axis=0, tiled=True).reshape(
        experts * capacity, -1
    )
    arrived = lax.all_gather(arrived, TP, axis=1, tiled=True)
    gate_act = jnp.dot(arrived, gate_local, preferred_element_type=jnp.float32)
    up_act = jnp.dot(arrived, up_local, preferred_element_type=jnp.float32)
    hidden = (jax.nn.silu(gate_act) * up_act).astype(jnp.bfloat16)
    down_local = expert_down[0]
    block_w = down_local
    expert_rows = summed_rows(
        lax.dot_general(
            block_w, hidden, (((0,), (1,)), ((), ())), preferred_element_type=jnp.float32
        ),
        TP,
    ).astype(jnp.bfloat16)
    returned = lax.all_to_all(
        expert_rows.reshape(expert_rows.shape[0], experts, capacity),
        "ep",
        split_axis=1,
        concat_axis=1,
        tiled=True,
    )
    returned_flat = returned.reshape(returned.shape[0], -1).astype(jnp.float32)
    moe_out = lax.dot_general(
        returned_flat,
        combine,
        (((1,), (1,)), ((), ())),
        precision=lax.Precision.HIGHEST,
        preferred_element_type=jnp.float32,
    )
    return (conv_out, moe_out.astype(jnp.bfloat16))


def solution(mesh):
    finer = Mesh(mesh.devices.reshape(mesh.shape["ep"], 8, 2), ("ep", "tp_0", "tp_1"))
    return jax.shard_map(
        body,
        mesh=finer,
        in_specs=(
            P("ep", None),
            P(),
            P(None, TP),
            P(None, TP),
            P(None, TP),
            P(TP),
            P(TP, None),
            P("ep", None),
            P(),
            P("ep", None),
            P("ep", None),
            P("ep", None, TP),
            P("ep", None, TP),
            P("ep", TP, None),
        ),
        out_specs=(P(TP, "ep"), P(TP, "ep")),
        check_vma=False,
    )
```

profile of v0, /device:TPU:8, one launch (start us, length us, event | category | flops | bytes accessed | tf_op | source)
XLA Modules:
  0.0 196.1 jit_solution(15484870692354183152)
XLA Ops:
  7.2 0.0 copy-start
  7.2 0.0 copy-start.1
  7.2 0.0 copy-start.6
  7.2 0.0 all-gather.2.cloned.1.call-start
  7.3 1.4 convert_element_type.61
  8.7 0.0 copy-done.1
  8.7 0.2 multiply_reduce_fusion
  8.9 0.0 copy-done.6
  8.9 0.1 copy.52
  9.0 0.1 eq.43
  9.2 0.1 eq.39
  9.3 0.9 reduce-window.6
  10.2 0.2 slice_reduce_fusion
  10.5 0.1 fusion.58
  10.6 0.1 reduce_sum.96
  10.8 0.1 mul.528
  10.9 2.9 %scatter_custom_fusion = s32[576]{0:T(1024)S(1)} fusion(s32[384]{0:T(512)S(1)} %fusion.70, s32[384]{0:T(512)S(1)} %fusion.64, s32[]{:T(128)} %constant.74.clone.1), kind=kCustom, calls=%fused_computation.130 | custom fusion | bytes 2308 | tf_op jit(solution)/shard_map/scatter | solution.py:119
  13.9 0.8 dynamic-slice
  14.7 0.1 fusion.25
  14.8 1.9 gather_fusion
  16.8 0.1 broadcast_in_dim.29
  16.9 0.1 broadcast_in_dim.50
  17.0 0.3 select_select_fusion
  17.3 24.6 %all_to_all.21 = bf16[32,18,128]{2,1,0:T(8,128)(2,1)S(1)} all-to-all(bf16[32,18,128]{2,1,0:T(8,128)(2,1)S(1)} %select_select_fusion), channel_id=1, replica_groups=mesh['ep'=32,'tp_0'=8,'tp_1'=2] {'ep'}, dimensions={0} | all-to-all | bytes 294912 | tf_op jit(solution)/shard_map/all_to_all | solution.py:136
  41.9 0.7 reshape.162
  42.6 0.0 all-gather.2.cloned.1.call-update
  42.7 0.0 reduce-scatter.5.cloned.1.call-start
  42.7 39.2 %all-gather.2.cloned.1.call-done = bf16[576,2048]{1,0:T(8,128)(2,1)} async-done(((bf16[576,128]{1,0:T(8,128)(2,1)}), bf16[576,2048]{1,0:T(8,128)(2,1)}) %all-gather.2.cloned.1.call-update) | async-done | bytes 2359312 | tf_op jit(solution)/shard_map/all_gather | solution.py:139
  81.9 3.8 %fusion.14 = f32[576,176]{0,1:T(8,128)} fusion(bf16[576,2048]{1,0:T(8,128)(2,1)} %all-gather.2.cloned.1.call-done, bf16[1,2048,176]{1,2,0:T(8,128)(2,1)} %param.25), kind=kOutput, calls=%fused_computation.26 | convolution fusion | flops 415236096 | bytes 3485696 | tf_op jit(solution)/shard_map/dot_general | solution.py:140
  85.7 0.0 copy-done
  85.7 0.0 copy-done.8
  85.7 4.7 %fusion = bf16[2048,576]{0,1:T(8,128)(2,1)} fusion(bf16[576,2048]{1,0:T(8,128)(2,1)S(1)} %copy-done.8, bf16[1,176,2048]{2,1,0:T(8,128)(2,1)S(1)} %copy-done, bf16[1,2048,176]{1,2,0:T(8,128)(2,1)} %param.26, f32[576,176]{0,1:T(8,128)} %fusion.14), kind=kOutput, calls=%fused_computation.3 | convolution fusion | flops 832260096 | bytes 6565888 | tf_op jit(solution)/shard_map/dot_general | solution.py:146
  90.4 0.0 reduce-scatter.5.cloned.1.call-update
  90.4 1.0 copy-done.3
  91.5 0.2 fusion.8
  91.7 0.0 copy-start.2
  91.7 0.0 copy-start.7
  91.7 0.4 fusion.5
  92.1 0.1 copy.48
  92.2 0.4 fusion.7
  92.6 3.4 %collective-permute-start = (bf16[128,30]{0,1:T(8,128)(2,1)S(1)}, bf16[128,30]{0,1:T(8,128)(2,1)S(1)}, u32[]{:S(2)}, u32[]{:S(2)}) collective-permute-start(bf16[128,30]{0,1:T(8,128)(2,1)S(1)} %slice.270), channel_id=1, source_target_pairs={{0,16},{16,32},{32,48},{48,64},{64,80},{80,96},{96,112},{112,128},... | collective-permute-start | bytes 23048 | tf_op jit(solution)/shard_map/ppermute | solution.py:14
  96.0 1.3 collective-permute-done
  97.3 0.3 fusion.76
  97.7 11.6 %all_to_all.22 = f32[16,1,256]{2,1,0:T(1,128)S(1)} all-to-all(f32[16,1,256]{2,1,0:T(1,128)S(1)} %broadcast_in_dim.28), channel_id=1, replica_groups=mesh['ep'=32,'tp_0'=8,'tp_1'=2] {'tp_0','tp_1'}, dimensions={0} | all-to-all | bytes 32768 | tf_op jit(solution)/shard_map/all_to_all | solution.py:19
  109.3 0.0 copy-done.7
  109.3 0.4 fusion.1
  109.7 0.9 copy.69
  110.6 4.8 %all-to-all-start.1 = ((bf16[16,128,128]{1,2,0:T(8,128)(2,1)}), bf16[16,128,128]{1,2,0:T(8,128)(2,1)S(1)}, u32[]{:S(2)}, u32[]{:S(2)}) async-start(bf16[16,128,128]{1,2,0:T(8,128)(2,1)} %bitcast.112), calls=%async_computation.1 | async-start | bytes 1048576 | tf_op jit(solution)/shard_map/all_to_all | solution.py:41
  115.5 0.0 reduce-scatter.7.cloned.1.call-start
  115.5 29.8 %reduce-scatter.5.cloned.1.call-done = bf16[256,576]{0,1:T(8,128)(2,1)} async-done(((bf16[2048,576]{0,1:T(8,128)(2,1)}), bf16[256,576]{0,1:T(8,128)(2,1)}) %reduce-scatter.5.cloned.1.call-update) | async-done | bytes 294928 | tf_op jit(solution)/shard_map/reduce_scatter | solution.py:48
  145.3 1.8 copy.59
  147.2 0.0 reduce-scatter.7.cloned.1.call-update
  147.2 0.1 copy.56
  147.3 17.1 %reduce-scatter.7.cloned.1.call-done = bf16[128,576]{1,0:T(8,128)(2,1)} async-done(((bf16[256,576]{1,0:T(8,128)(2,1)}), bf16[128,576]{1,0:T(8,128)(2,1)}) %reduce-scatter.7.cloned.1.call-update) | async-done | bytes 147472
  164.4 1.1 copy.60
  165.5 0.7 reshape.163
  166.2 0.0 all-to-all-done.1
  166.2 10.2 %all-to-all-start.3 = ((bf16[128,32,18]{0,2,1:T(8,128)(2,1)}), bf16[128,32,18]{0,2,1:T(8,128)(2,1)S(1)}, u32[]{:S(2)}, u32[]{:S(2)}) async-start(bf16[128,32,18]{0,2,1:T(8,128)(2,1)} %reshape.163), calls=%async_computation.4 | async-start | bytes 393216 | tf_op jit(solution)/shard_map/all_to_all | solution.py:151
  176.4 0.2 select_reduce_fusion
  176.6 0.1 reduce_sum.92
  176.7 0.7 copy.57
  177.4 11.1 %all-to-all-done.3 = bf16[128,32,18]{0,2,1:T(8,128)(2,1)S(1)} async-done(((bf16[128,32,18]{0,2,1:T(8,128)(2,1)}), bf16[128,32,18]{0,2,1:T(8,128)(2,1)S(1)}, u32[]{:S(2)}, u32[]{:S(2)}) %all-to-all-start.3) | async-done | bytes 147488 | tf_op jit(solution)/shard_map/all_to_all | solution.py:151
  188.6 0.1 reshape.164
  188.6 1.0 convolution_convert_fusion.2
  (35 shorter events, 0.4 us)
Async XLA Ops:
  7.2 78.5 %copy-start = (bf16[1,176,2048]{2,1,0:T(8,128)(2,1)S(1)}, bf16[1,176,2048]{2,1,0:T(8,128)(2,1)}, u32[]{:S(2)}) copy-start(bf16[1,176,2048]{2,1,0:T(8,128)(2,1)} %param.27) | copy-start | bytes 2162692
  7.2 1.5 copy-start.1
  7.2 1.7 copy-start.6
  7.2 74.7 %all-gather.2.cloned.1.call-start = ((), (), s32[]{:S(2)}) async-start(), calls=%async_computation.6 | async-start | bytes 2506752 | tf_op jit(solution)/shard_map/all_gather | solution.py:139
  42.7 102.7 %reduce-scatter.5.cloned.1.call-start = ((), (), s32[]{:S(2)}) async-start(), calls=%async_computation.7 | async-start | bytes 2654208 | tf_op jit(solution)/shard_map/reduce_scatter | solution.py:48
  81.9 3.8 %copy-start.8 = (bf16[576,2048]{1,0:T(8,128)(2,1)S(1)}, bf16[576,2048]{1,0:T(8,128)(2,1)}, u32[]{:S(2)}) copy-start(bf16[576,2048]{1,0:T(8,128)(2,1)} %all-gather.2.cloned.1.call-done) | copy-start | bytes 7077892
  90.4 1.0 copy-start.3
  90.4 1.2 copy-start.9
  90.4 1.2 copy-start.11
  90.4 1.8 copy-start.10
  91.5 4.5 %copy-start.5 = (f32[31,128]{1,0:T(8,128)S(1)}, f32[31,128]{1,0:T(8,128)}, u32[]{:S(2)}) copy-start(f32[31,128]{1,0:T(8,128)} %param.18) | copy-start | bytes 47620
  91.7 17.6 %copy-start.2 = (bf16[128,2048]{1,0:T(8,128)(2,1)S(1)}, bf16[128,2048]{1,0:T(8,128)(2,1)}, u32[]{:S(2)}) copy-start(bf16[128,2048]{1,0:T(8,128)(2,1)} %param.20) | copy-start | bytes 1572868
  91.7 17.6 %copy-start.7 = (f32[128]{0:T(128)S(1)}, f32[128]{0:T(128)}, u32[]{:S(2)}) copy-start(f32[128]{0:T(128)} %param.19) | copy-start | bytes 1540
  92.6 4.7 %collective-permute-start = (bf16[128,30]{0,1:T(8,128)(2,1)S(1)}, bf16[128,30]{0,1:T(8,128)(2,1)S(1)}, u32[]{:S(2)}, u32[]{:S(2)}) collective-permute-start(bf16[128,30]{0,1:T(8,128)(2,1)S(1)} %slice.270), channel_id=1, source_target_pairs={{0,16},{16,32},{32,48},{48,64},{64,80},{80,96},{96,112},{112,128},... | collective-permute-start | bytes 23048 | tf_op jit(solution)/shard_map/ppermute | solution.py:14
  97.6 49.7 %copy-start.4 = (f32[192,2]{0,1:T(2,128)S(1)}, f32[192,2]{0,1:T(2,128)}, u32[]{:S(2)}) copy-start(f32[192,2]{0,1:T(2,128)} %param.24) | copy-start | bytes 4612
  110.6 55.6 %all-to-all-start.1 = ((bf16[16,128,128]{1,2,0:T(8,128)(2,1)}), bf16[16,128,128]{1,2,0:T(8,128)(2,1)S(1)}, u32[]{:S(2)}, u32[]{:S(2)}) async-start(bf16[16,128,128]{1,2,0:T(8,128)(2,1)} %bitcast.112), calls=%async_computation.1 | async-start | bytes 1048576 | tf_op jit(solution)/shard_map/all_to_all | solution.py:41
  115.5 49.0 %reduce-scatter.7.cloned.1.call-start = ((), (), s32[]{:S(2)}) async-start(), calls=%async_computation.8 | async-start | bytes 491520
  166.2 22.3 %all-to-all-start.3 = ((bf16[128,32,18]{0,2,1:T(8,128)(2,1)}), bf16[128,32,18]{0,2,1:T(8,128)(2,1)S(1)}, u32[]{:S(2)}, u32[]{:S(2)}) async-start(bf16[128,32,18]{0,2,1:T(8,128)(2,1)} %reshape.163), calls=%async_computation.4 | async-start | bytes 393216 | tf_op jit(solution)/shard_map/all_to_all | solution.py:151
Sparse Core Ops, SparseCore 0:
  42.8 39.1 all-gather.1
  90.6 54.7 reduce-scatter.4
  148.1 16.2 reduce-scatter.6
where the time goes:
time: 197 us; the launch traced here: 196 us
  waiting for transfers between devices  98.6 us (50%)
  blocking collectives  36.2 us (18%)
  starting transfers between devices  18.5 us (9%)
  local copies, waits for them, and re-layouts  14.1 us (7%)
  between operations  14.1 us (7%)
  matrix products  10.6 us (5%)
  other arithmetic  3.98 us (2%)
    all_gather x1, waiting for transfers between devices, body(): arrived = lax.all_gather(arrived, TP, axis=1, tiled=True)  39.2 us
    reduce_scatter x1, waiting for transfers between devices, summed_rows(): so_far = lax.psum_scatter(so_far, axis, scatter_dimension=0, tiled=True)  29.8 us
    all_to_all x1, blocking collectives, body(): lax.all_to_all(send_rows, 'ep', split_axis=0, concat_axis=0, tiled=True)  24.6 us
    unnamed x4, waiting for transfers between devices  17.2 us
    all_to_all x1, blocking collectives, copy_for_each(): lax.all_to_all(jnp.broadcast_to(x[None], (peers, *x.shape)), axis, 0, 0,...  11.6 us
    all_to_all x1, waiting for transfers between devices, body(): lax.all_to_all(expert_rows.reshape(expert_rows.shape[0], experts, capacit...  11.1 us
    all_to_all x1, starting transfers between devices, body(): lax.all_to_all(expert_rows.reshape(expert_rows.shape[0], experts, capacit...  10.2 us
    all_to_all x1, starting transfers between devices, sum_at_owner(): tiles = lax.all_to_all(in_blocks(x, dim, peers), axis, 0, 0, tiled=True)  4.82 us
  transfers between devices with their start and end apart: 6, of which 5 were waited for; matrix products, arithmetic and copies ran while one was open for 4% of the time, Pallas kernels for 0%

commit v1 on v0

--- a/solution.py
+++ b/solution.py
@@ -6,6 +6,9 @@
 
 CONV_CH = 2048
 TP = ("tp_0", "tp_1")
+advance_boxes = lambda x_part, ax_name: jnp.concatenate(
+    lax.all_to_all(jnp.stack(lax.axis_size(ax_name) * [x_part], axis=0), ax_name, 0, 0), 1
+)
 
 
 def from_behind(block, axis, distance):
@@ -136,7 +139,7 @@
     arrived = lax.all_to_all(send_rows, "ep", split_axis=0, concat_axis=0, tiled=True).reshape(
         experts * capacity, -1
     )
-    arrived = lax.all_gather(arrived, TP, axis=1, tiled=True)
+    arrived = advance_boxes(arrived, TP)
     gate_act = jnp.dot(arrived, gate_local, preferred_element_type=jnp.float32)
     up_act = jnp.dot(arrived, up_local, preferred_element_type=jnp.float32)
     hidden = (jax.nn.silu(gate_act) * up_act).astype(jnp.bfloat16)

time: 197 us -> 211 us (1.071)
  blocking collectives: 36.2 us -> 97.9 us
  waiting for transfers between devices: 98.6 us -> 54.3 us
    all_to_all x0 -> x1, blocking collectives: none -> 62.2 us  [lax.all_to_all(jnp.stack(lax.axis_size(ax_name) * [x_part], axis=0), ax_n...]
    all_gather x1 -> x0, waiting for transfers between devices: 39.2 us -> none  [body(): arrived = lax.all_gather(arrived, TP, axis=1, tiled=True)]
    reduce_scatter x1, waiting for transfers between devices: 29.8 us -> 24.3 us  [summed_rows(): so_far = lax.psum_scatter(so_far, axis, scatter_dimension=0, tiled=True)]
    unnamed x4 -> x3, waiting for transfers between devices: 17.2 us -> 17.5 us
  transfers between devices with their start and end apart: 6 -> 5, of which waited for: 5 -> 4; matrix products, arithmetic and copies ran while one was open for 4% -> 4% of each run, Pallas kernels for 0% -> 0%
where the time goes in v1:
time: 211 us; the launch traced here: 210 us
  blocking collectives  97.9 us (46%)
  waiting for transfers between devices  54.3 us (26%)
  starting transfers between devices  17 us (8%)
  between operations  14.4 us (7%)
  local copies, waits for them, and re-layouts  13.9 us (7%)
  matrix products  8.58 us (4%)
  other arithmetic  3.98 us (2%)
    all_to_all x1, blocking collectives, lax.all_to_all(jnp.stack(lax.axis_size(ax_name) * [x_part], axis=0), ax_n...  62.2 us
    all_to_all x1, blocking collectives, body(): lax.all_to_all(send_rows, 'ep', split_axis=0, concat_axis=0, tiled=True)  24.6 us
    reduce_scatter x1, waiting for transfers between devices, summed_rows(): so_far = lax.psum_scatter(so_far, axis, scatter_dimension=0, tiled=True)  24.3 us
    unnamed x3, waiting for transfers between devices  17.5 us
    all_to_all x1, waiting for transfers between devices, body(): lax.all_to_all(expert_rows.reshape(expert_rows.shape[0], experts, capacit...  11.1 us
    all_to_all x1, blocking collectives, copy_for_each(): lax.all_to_all(jnp.broadcast_to(x[None], (peers, *x.shape)), axis, 0, 0,...  11.1 us
    all_to_all x1, starting transfers between devices, body(): lax.all_to_all(expert_rows.reshape(expert_rows.shape[0], experts, capacit...  10.2 us
    all_to_all x1, starting transfers between devices, sum_at_owner(): tiles = lax.all_to_all(in_blocks(x, dim, peers), axis, 0, 0, tiled=True)  4.87 us
  transfers between devices with their start and end apart: 5, of which 4 were waited for; matrix products, arithmetic and copies ran while one was open for 4% of the time, Pallas kernels for 0%

profile of v1, /device:TPU:8, one launch (start us, length us, event | category | flops | bytes accessed | tf_op | source)
XLA Modules:
  0.0 210.1 jit_solution(12220497322713236495)
XLA Ops:
  7.2 0.0 copy-start
  7.2 0.0 copy-start.1
  7.2 0.0 reduce-scatter.5.cloned.1.call-start
  7.2 1.4 convert_element_type.61
  8.7 0.0 copy-done.1
  8.7 0.2 multiply_reduce_fusion
  8.9 0.0 copy-done.6
  8.9 0.1 copy.54
  9.0 0.1 eq.43
  9.2 0.1 eq.39
  9.3 0.9 reduce-window.6
  10.2 0.2 slice_reduce_fusion
  10.5 0.1 fusion.70
  10.6 0.1 reduce_sum.96
  10.8 0.1 mul.528
  10.9 2.9 %scatter_custom_fusion = s32[576]{0:T(1024)S(1)} fusion(s32[384]{0:T(512)S(1)} %fusion.82, s32[384]{0:T(512)S(1)} %fusion.76, s32[]{:T(128)} %constant.74.clone.1), kind=kCustom, calls=%fused_computation.135 | custom fusion | bytes 2308 | tf_op jit(solution)/shard_map/scatter | solution.py:122
  13.9 0.8 dynamic-slice
  14.7 0.1 fusion.37
  14.8 1.9 gather_fusion
  16.8 0.1 broadcast_in_dim.29
  16.9 0.1 broadcast_in_dim.50
  17.0 0.3 select_select_fusion
  17.3 24.6 %all_to_all.26 = bf16[32,18,128]{2,1,0:T(8,128)(2,1)S(1)} all-to-all(bf16[32,18,128]{2,1,0:T(8,128)(2,1)S(1)} %select_select_fusion), channel_id=1, replica_groups=mesh['ep'=32,'tp_0'=8,'tp_1'=2] {'ep'}, dimensions={0} | all-to-all | bytes 294912 | tf_op jit(solution)/shard_map/all_to_all | solution.py:139
  41.9 0.1 stack_reshape.2
  42.0 0.4 stack.3
  42.4 0.0 copy-start.8
  42.4 62.2 %all_to_all.27 = bf16[16,576,128]{2,1,0:T(8,128)(2,1)S(1)} all-to-all(bf16[16,576,128]{2,1,0:T(8,128)(2,1)S(1)} %stack.3), channel_id=1, replica_groups=mesh['ep'=32,'tp_0'=8,'tp_1'=2] {'tp_0','tp_1'}, dimensions={0} | all-to-all | bytes 4718592 | tf_op jit(solution)/shard_map/all_to_all | solution.py:10
  104.6 1.8 fusion.3
  106.4 0.0 copy-done
  106.4 4.7 %fusion = bf16[2048,576]{0,1:T(8,128)(2,1)} fusion(bf16[1,176,2048]{2,1,0:T(8,128)(2,1)S(1)} %copy-done, bf16[1,2048,176]{1,2,0:T(8,128)(2,1)} %param.26, f32[576,176]{0,1:T(8,128)} %fusion.3, bf16[16,576,128]{2,1,0:T(8,128)(2,1)S(1)} %all_to_all.27), kind=kOutput, calls=%fused_computation.3 | convolution fusion | flops 832260096 | bytes 6565888 | tf_op jit(solution)/shard_map/dot_general | solution.py:149
  111.1 0.0 reduce-scatter.5.cloned.1.call-update
  111.2 1.0 copy-done.3
  112.2 0.2 fusion.21
  112.4 0.0 copy-start.2
  112.4 0.0 copy-start.7
  112.4 0.4 fusion.18
  112.8 0.1 copy.50
  112.9 0.4 fusion.20
  113.3 1.9 collective-permute-start
  115.2 0.0 copy-done.5
  115.2 1.3 collective-permute-done
  116.6 0.3 fusion.88
  116.8 0.0 copy-start.4
  116.9 11.1 %all_to_all.28 = f32[16,1,256]{2,1,0:T(1,128)S(1)} all-to-all(f32[16,1,256]{2,1,0:T(1,128)S(1)} %broadcast_in_dim.28), channel_id=1, replica_groups=mesh['ep'=32,'tp_0'=8,'tp_1'=2] {'tp_0','tp_1'}, dimensions={0} | all-to-all | bytes 32768 | tf_op jit(solution)/shard_map/all_to_all | solution.py:22
  128.0 0.4 fusion.7
  128.4 0.9 copy.87
  129.3 4.9 %all-to-all-start.1 = ((bf16[16,128,128]{1,2,0:T(8,128)(2,1)}), bf16[16,128,128]{1,2,0:T(8,128)(2,1)S(1)}, u32[]{:S(2)}, u32[]{:S(2)}) async-start(bf16[16,128,128]{1,2,0:T(8,128)(2,1)} %bitcast.130), calls=%async_computation.1 | async-start | bytes 1048576 | tf_op jit(solution)/shard_map/all_to_all | solution.py:44
  134.2 0.0 reduce-scatter.7.cloned.1.call-start
  134.3 24.3 %reduce-scatter.5.cloned.1.call-done = bf16[256,576]{0,1:T(8,128)(2,1)} async-done(((bf16[2048,576]{0,1:T(8,128)(2,1)}), bf16[256,576]{0,1:T(8,128)(2,1)}) %reduce-scatter.5.cloned.1.call-update) | async-done | bytes 294928 | tf_op jit(solution)/shard_map/reduce_scatter | solution.py:51
  158.6 1.8 copy.62
  160.4 0.0 reduce-scatter.7.cloned.1.call-update
  160.5 0.1 copy.59
  160.5 0.0 copy-done.4
  160.6 17.5 %reduce-scatter.7.cloned.1.call-done = bf16[128,576]{1,0:T(8,128)(2,1)} async-done(((bf16[256,576]{1,0:T(8,128)(2,1)}), bf16[128,576]{1,0:T(8,128)(2,1)}) %reduce-scatter.7.cloned.1.call-update) | async-done | bytes 147472
  178.1 1.1 copy.63
  179.1 0.7 reshape.169
  179.9 0.0 all-to-all-done.1
  179.9 10.2 %all-to-all-start.4 = ((bf16[128,32,18]{0,2,1:T(8,128)(2,1)}), bf16[128,32,18]{0,2,1:T(8,128)(2,1)S(1)}, u32[]{:S(2)}, u32[]{:S(2)}) async-start(bf16[128,32,18]{0,2,1:T(8,128)(2,1)} %reshape.169), calls=%async_computation.5 | async-start | bytes 393216 | tf_op jit(solution)/shard_map/all_to_all | solution.py:154
  190.1 0.2 select_reduce_fusion
  190.3 0.1 reduce_sum.92
  190.4 0.7 copy.60
  191.1 11.1 %all-to-all-done.4 = bf16[128,32,18]{0,2,1:T(8,128)(2,1)S(1)} async-done(((bf16[128,32,18]{0,2,1:T(8,128)(2,1)}), bf16[128,32,18]{0,2,1:T(8,128)(2,1)S(1)}, u32[]{:S(2)}, u32[]{:S(2)}) %all-to-all-start.4) | async-done | bytes 147488 | tf_op jit(solution)/shard_map/all_to_all | solution.py:154
  202.2 0.1 reshape.170
  202.3 1.0 convolution_convert_fusion.2
  (34 shorter events, 0.4 us)
Async XLA Ops:
  7.2 99.2 %copy-start = (bf16[1,176,2048]{2,1,0:T(8,128)(2,1)S(1)}, bf16[1,176,2048]{2,1,0:T(8,128)(2,1)}, u32[]{:S(2)}) copy-start(bf16[1,176,2048]{2,1,0:T(8,128)(2,1)} %param.27) | copy-start | bytes 2162692
  7.2 1.5 copy-start.1
  7.2 1.7 copy-start.6
  7.2 151.4 %reduce-scatter.5.cloned.1.call-start = ((), (), s32[]{:S(2)}) async-start(), calls=%async_computation.7 | async-start | bytes 2654208 | tf_op jit(solution)/shard_map/reduce_scatter | solution.py:51
  42.4 62.2 %copy-start.8 = (bf16[1,2048,176]{1,2,0:T(8,128)(2,1)S(1)}, bf16[1,2048,176]{1,2,0:T(8,128)(2,1)}, u32[]{:S(2)}) copy-start(bf16[1,2048,176]{1,2,0:T(8,128)(2,1)} %param.25) | copy-start | bytes 2162692
  111.1 1.0 copy-start.3
  111.1 1.2 copy-start.9
  111.1 1.2 copy-start.11
  111.1 1.8 copy-start.10
  112.2 3.0 %copy-start.5 = (f32[31,128]{1,0:T(8,128)S(1)}, f32[31,128]{1,0:T(8,128)}, u32[]{:S(2)}) copy-start(f32[31,128]{1,0:T(8,128)} %param.18) | copy-start | bytes 47620
  112.4 15.6 %copy-start.2 = (bf16[128,2048]{1,0:T(8,128)(2,1)S(1)}, bf16[128,2048]{1,0:T(8,128)(2,1)}, u32[]{:S(2)}) copy-start(bf16[128,2048]{1,0:T(8,128)(2,1)} %param.20) | copy-start | bytes 1572868
  112.4 15.6 %copy-start.7 = (f32[128]{0:T(128)S(1)}, f32[128]{0:T(128)}, u32[]{:S(2)}) copy-start(f32[128]{0:T(128)} %param.19) | copy-start | bytes 1540
  113.3 3.2 %collective-permute-start = (bf16[128,30]{0,1:T(8,128)(2,1)S(1)}, bf16[128,30]{0,1:T(8,128)(2,1)S(1)}, u32[]{:S(2)}, u32[]{:S(2)}) collective-permute-start(bf16[128,30]{0,1:T(8,128)(2,1)S(1)} %slice.270), channel_id=1, source_target_pairs={{0,16},{16,32},{32,48},{48,64},{64,80},{80,96},{96,112},{112,128},... | collective-permute-start | bytes 23048 | tf_op jit(solution)/shard_map/ppermute | solution.py:17
  116.8 43.7 %copy-start.4 = (f32[192,2]{0,1:T(2,128)S(1)}, f32[192,2]{0,1:T(2,128)}, u32[]{:S(2)}) copy-start(f32[192,2]{0,1:T(2,128)} %param.24) | copy-start | bytes 4612
  129.3 50.5 %all-to-all-start.1 = ((bf16[16,128,128]{1,2,0:T(8,128)(2,1)}), bf16[16,128,128]{1,2,0:T(8,128)(2,1)S(1)}, u32[]{:S(2)}, u32[]{:S(2)}) async-start(bf16[16,128,128]{1,2,0:T(8,128)(2,1)} %bitcast.130), calls=%async_computation.1 | async-start | bytes 1048576 | tf_op jit(solution)/shard_map/all_to_all | solution.py:44
  134.2 43.9 %reduce-scatter.7.cloned.1.call-start = ((), (), s32[]{:S(2)}) async-start(), calls=%async_computation.8 | async-start | bytes 491520
  179.9 22.4 %all-to-all-start.4 = ((bf16[128,32,18]{0,2,1:T(8,128)(2,1)}), bf16[128,32,18]{0,2,1:T(8,128)(2,1)S(1)}, u32[]{:S(2)}, u32[]{:S(2)}) async-start(bf16[128,32,18]{0,2,1:T(8,128)(2,1)} %reshape.169), calls=%async_computation.5 | async-start | bytes 393216 | tf_op jit(solution)/shard_map/all_to_all | solution.py:154
Sparse Core Ops, SparseCore 0:
  111.3 47.2 reduce-scatter.4
  161.4 16.6 reduce-scatter.6
